TPU v7x, 32 devices: a whole 2x2x4 slice. The times are simulated.
32 devices in a mesh: fs: 16 (over z, y, x), tp: 2 (over core).
Axes of the slice: x: 2, y: 2, z: 4, core: 2. Of those that a mesh axis runs over, the one named last changes fastest.
Arguments:
- tokens: bfloat16 [6144, 2048], P('fs'), may hold values from -6 to 6
- merged: bfloat16 [6144, 2048], P('fs'), may hold values from -6 to 6
- gain_first: float32 [2048], replicated, may hold values from 0.1 to 1.9
- gate_first: bfloat16 [2048, 2816], P('fs', 'tp'), may hold values from -0.125 to 0.125
- up_first: bfloat16 [2048, 2816], P('fs', 'tp'), may hold values from -0.125 to 0.125
- down_first: bfloat16 [2816, 2048], P('tp', 'fs'), may hold values from -0.21875 to 0.21875
- gain_second: float32 [2048], replicated, may hold values from 0.1 to 1.9
- gate_second: bfloat16 [2048, 2816], P('fs', 'tp'), may hold values from -0.125 to 0.125
- up_second: bfloat16 [2048, 2816], P('fs', 'tp'), may hold values from -0.125 to 0.125
- down_second: bfloat16 [2816, 2048], P('tp', 'fs'), may hold values from -0.21875 to 0.21875
Outputs:
- result: bfloat16 [6144, 2048], P('fs')
All inputs are finite; a program needn't handle non-finite values.
Results may differ from a plain program's by a relative error of at most 0.01.
Values may be sent and summed in bfloat16 or wider, within the bound.
A program may use at most 64 MiB of HBM per device.

v0:
```python
import jax
import jax.numpy as jnp
from jax import lax
from jax.sharding import PartitionSpec as P

EPS = 1e-06


def norm_rows(values, gain):
    scale = lax.rsqrt(jnp.mean(values * values, axis=-1, keepdims=True) + EPS)
    return values * scale * gain


def make_folder(normed, pieces):
    return (
        jnp.dot(normed, pieces[0], preferred_element_type=jnp.float32),
        jnp.dot(normed, pieces[1], preferred_element_type=jnp.float32),
    )


def shards(
    tokens,
    merged,
    gain_first,
    gate_first,
    up_first,
    down_first,
    gain_second,
    gate_second,
    up_second,
    down_second,
):
    normed_first = norm_rows(tokens.astype(jnp.float32), gain_first).astype(jnp.bfloat16)
    gate, up = make_folder(
        normed_first,
        (
            lax.all_gather(gate_first, "fs", axis=0, tiled=True),
            lax.all_gather(up_first, "fs", axis=0, tiled=True),
        ),
    )
    hidden = (jax.nn.silu(gate) * up).astype(jnp.bfloat16)
    down_whole = lax.all_gather(down_first, "fs", axis=1, tiled=True)
    partial_value = jnp.dot(hidden, down_whole, preferred_element_type=jnp.float32)
    first_sum = lax.psum(partial_value.astype(jnp.bfloat16), "tp").astype(jnp.float32)
    middle = tokens.astype(jnp.float32) + merged.astype(jnp.float32) + 0.5 * first_sum
    normed_second = norm_rows(middle, gain_second).astype(jnp.bfloat16)
    gate_two, up_two = make_folder(
        normed_second,
        (
            lax.all_gather(gate_second, "fs", axis=0, tiled=True),
            lax.all_gather(up_second, "fs", axis=0, tiled=True),
        ),
    )
    hidden_two = (jax.nn.silu(gate_two) * up_two).astype(jnp.bfloat16)
    down_two = lax.all_gather(down_second, "fs", axis=1, tiled=True)
    partial_two = jnp.dot(hidden_two, down_two, preferred_element_type=jnp.float32)
    second_sum = lax.psum(partial_two.astype(jnp.bfloat16), "tp").astype(jnp.float32)
    return (middle + 0.5 * second_sum).astype(jnp.bfloat16)


def solution(mesh):
    return jax.shard_map(
        shards,
        mesh=mesh,
        in_specs=(
            P("fs", None),
            P("fs", None),
            P(),
            P("fs", "tp"),
            P("fs", "tp"),
            P("tp", "fs"),
            P(),
            P("fs", "tp"),
            P("fs", "tp"),
            P("tp", "fs"),
        ),
        out_specs=P("fs", None),
        check_vma=False,
    )
```

profile of v0, /device:TPU:0, one launch (start us, length us, event | category | flops | bytes accessed | tf_op | source)
XLA Modules:
  0.0 665.2 jit_solution(4083028435205835512)
XLA Ops:
  6.5 0.7 all-gather.7.cloned.1.call-update
  7.3 0.7 all-gather.11.cloned.1.call-update
  8.1 0.7 all-gather.9.cloned.1.call-update
  8.8 1.8 fusion.1
  10.6 90.9 %all-gather.7.cloned.1.call-done = bf16[2048,1408]{1,0:T(8,128)(2,1)} async-done(((bf16[128,1408]{1,0:T(8,128)(2,1)}), bf16[2048,1408]{1,0:T(8,128)(2,1)}) %all-gather.7.cloned.1.call-update) | async-done | bytes 5767184 | tf_op jit(solution)/shard_map/all_gather | solution.py:37
  101.5 7.1 %fusion.8 = f32[384,1408]{1,0:T(8,128)} fusion(bf16[2048,1408]{1,0:T(8,128)(2,1)} %all-gather.7.cloned.1.call-done, bf16[384,2048]{1,0:T(8,128)(2,1)} %param.10, f32[2048]{0:T(1024)} %param.12, f32[384]{0:T(512)S(1)} %add_rsqrt_fusion.1), kind=kOutput, calls=%fused_computation.16 | convolution fusion | flops 2217738240 | bytes 9512448 | tf_op jit(solution)/shard_map/dot_general | solution.py:16
  108.7 102.6 %all-gather.11.cloned.1.call-done = bf16[1408,2048]{1,0:T(8,128)(2,1)} async-done(((bf16[1408,128]{1,0:T(8,128)(2,1)}), bf16[1408,2048]{1,0:T(8,128)(2,1)}) %all-gather.11.cloned.1.call-update) | async-done | bytes 5767184 | tf_op jit(solution)/shard_map/all_gather | solution.py:42
  211.3 89.7 %all-gather.9.cloned.1.call-done = bf16[2048,1408]{1,0:T(8,128)(2,1)} async-done(((bf16[128,1408]{1,0:T(8,128)(2,1)}), bf16[2048,1408]{1,0:T(8,128)(2,1)}) %all-gather.9.cloned.1.call-update) | async-done | bytes 5767184 | tf_op jit(solution)/shard_map/all_gather | solution.py:38
  300.9 11.2 %convolution_convert_fusion.1 = bf16[384,2048]{1,0:T(8,128)(2,1)} fusion(bf16[1408,2048]{1,0:T(8,128)(2,1)} %all-gather.11.cloned.1.call-done, bf16[2048,1408]{1,0:T(8,128)(2,1)} %all-gather.9.cloned.1.call-done, f32[384,1408]{1,0:T(8,128)} %fusion.8, bf16[384,2048]{1,0:T(8,128)(2,1)S(1)} %copy-done, f32[2048]{0:T(1024)S(1)} %copy-done.4, ...), kind=kOutput, calls=%fused_computation.15 | convolution fusion | flops 4436361216 | bytes 16852480 | tf_op jit(solution)/shard_map/dot_general | solution.py:43
  312.2 0.0 all-gather.13.cloned.1.call-start
  312.2 0.5 all-gather.13.cloned.1.call-update
  312.8 0.5 all-gather.15.cloned.1.call-update
  313.4 0.7 all-gather.17.cloned.1.call-update
  314.1 0.2 all-reduce.5.cloned.1.call-start
  314.3 17.0 %all-reduce.3.cloned.1.call-done = bf16[384,2048]{1,0:T(8,128)(2,1)} async-done(((bf16[384,2048]{1,0:T(8,128)(2,1)}), bf16[384,2048]{1,0:T(8,128)(2,1)}) %all-reduce.3.cloned.1.call-update) | async-done | bytes 1572880 | tf_op jit(solution)/shard_map/psum | solution.py:44
  331.3 2.4 multiply_reduce_fusion
  333.8 2.2 multiply_convert_fusion
  336.0 87.8 %all-gather.13.cloned.1.call-done = bf16[2048,1408]{1,0:T(8,128)(2,1)} async-done(((bf16[128,1408]{1,0:T(8,128)(2,1)}), bf16[2048,1408]{1,0:T(8,128)(2,1)}) %all-gather.13.cloned.1.call-update) | async-done | bytes 5767184 | tf_op jit(solution)/shard_map/all_gather | solution.py:50
  423.8 7.1 %fusion.12 = f32[384,1408]{1,0:T(8,128)} fusion(bf16[384,2048]{1,0:T(8,128)(2,1)} %multiply_convert_fusion, bf16[2048,1408]{1,0:T(8,128)(2,1)} %all-gather.13.cloned.1.call-done), kind=kOutput, calls=%fused_computation.21 | convolution fusion | flops 2214592512 | bytes 9502720 | tf_op jit(solution)/shard_map/dot_general | solution.py:16
  430.9 82.9 %all-gather.15.cloned.1.call-done = bf16[2048,1408]{1,0:T(8,128)(2,1)} async-done(((bf16[128,1408]{1,0:T(8,128)(2,1)}), bf16[2048,1408]{1,0:T(8,128)(2,1)}) %all-gather.15.cloned.1.call-update) | async-done | bytes 5767184 | tf_op jit(solution)/shard_map/all_gather | solution.py:51
  513.8 109.7 %all-gather.17.cloned.1.call-done = bf16[1408,2048]{1,0:T(8,128)(2,1)} async-done(((bf16[1408,128]{1,0:T(8,128)(2,1)}), bf16[1408,2048]{1,0:T(8,128)(2,1)}) %all-gather.17.cloned.1.call-update) | async-done | bytes 5767184 | tf_op jit(solution)/shard_map/all_gather | solution.py:55
  623.6 11.7 %convolution_convert_fusion = bf16[384,2048]{1,0:T(8,128)(2,1)} fusion(bf16[1408,2048]{1,0:T(8,128)(2,1)} %all-gather.17.cloned.1.call-done, bf16[384,2048]{1,0:T(8,128)(2,1)} %multiply_convert_fusion, bf16[2048,1408]{1,0:T(8,128)(2,1)} %all-gather.15.cloned.1.call-done, f32[384,1408]{1,0:T(8,128)} %fusion.12), kind=kOutput, calls=%fused_computation.14 | convolution fusion | flops 4433215488 | bytes 16842752 | tf_op jit(solution)/shard_map/dot_general | solution.py:56
  635.3 18.7 %all-reduce.5.cloned.1.call-done = bf16[384,2048]{1,0:T(8,128)(2,1)} async-done(((bf16[384,2048]{1,0:T(8,128)(2,1)}), bf16[384,2048]{1,0:T(8,128)(2,1)}) %all-reduce.5.cloned.1.call-update) | async-done | bytes 1572880 | tf_op jit(solution)/shard_map/psum | solution.py:57
  654.0 4.3 add_convert_fusion
  (20 shorter events, 0.3 us)
Async XLA Ops:
  6.5 95.0 %all-gather.7.cloned.1.call-start = ((), (), s32[]{:S(2)}) async-start(), calls=%async_computation | async-start | bytes 6127616 | tf_op jit(solution)/shard_map/all_gather | solution.py:37
  7.3 204.0 %all-gather.11.cloned.1.call-start = ((), (), s32[]{:S(2)}) async-start(), calls=%async_computation.2 | async-start | bytes 6127616 | tf_op jit(solution)/shard_map/all_gather | solution.py:42
  8.0 292.9 %all-gather.9.cloned.1.call-start = ((), (), s32[]{:S(2)}) async-start(), calls=%async_computation.1 | async-start | bytes 6127616 | tf_op jit(solution)/shard_map/all_gather | solution.py:38
  8.7 322.6 %all-reduce.3.cloned.1.call-start = ((), (), s32[]{:S(2)}) async-start(), calls=%async_computation.3 | async-start | bytes 3145728 | tf_op jit(solution)/shard_map/psum | solution.py:44
  10.6 290.3 %copy-start = (bf16[384,2048]{1,0:T(8,128)(2,1)S(1)}, bf16[384,2048]{1,0:T(8,128)(2,1)}, u32[]{:S(2)}) copy-start(bf16[384,2048]{1,0:T(8,128)(2,1)} %param.10) | copy-start | bytes 4718596
  10.6 290.3 %copy-start.4 = (f32[2048]{0:T(1024)S(1)}, f32[2048]{0:T(1024)}, u32[]{:S(2)}) copy-start(f32[2048]{0:T(1024)} %param.12) | copy-start | bytes 24580
  312.1 19.2 %copy-start.1 = (bf16[384,2048]{1,0:T(8,128)(2,1)S(1)}, bf16[384,2048]{1,0:T(8,128)(2,1)}, u32[]{:S(2)}) copy-start(bf16[384,2048]{1,0:T(8,128)(2,1)} %param.11) | copy-start | bytes 4718596
  312.2 21.6 %copy-start.3 = (f32[2048]{0:T(1024)S(1)}, f32[2048]{0:T(1024)}, u32[]{:S(2)}) copy-start(f32[2048]{0:T(1024)} %param.16) | copy-start | bytes 24580
  312.2 111.7 %all-gather.13.cloned.1.call-start = ((), (), s32[]{:S(2)}) async-start(), calls=%async_computation.4 | async-start | bytes 6127616 | tf_op jit(solution)/shard_map/all_gather | solution.py:50
  312.8 201.1 %all-gather.15.cloned.1.call-start = ((), (), s32[]{:S(2)}) async-start(), calls=%async_computation.5 | async-start | bytes 6127616 | tf_op jit(solution)/shard_map/all_gather | solution.py:51
  313.3 310.2 %all-gather.17.cloned.1.call-start = ((), (), s32[]{:S(2)}) async-start(), calls=%async_computation.6 | async-start | bytes 6127616 | tf_op jit(solution)/shard_map/all_gather | solution.py:55
  314.1 340.0 %all-reduce.5.cloned.1.call-start = ((), (), s32[]{:S(2)}) async-start(), calls=%async_computation.7 | async-start | bytes 3145728 | tf_op jit(solution)/shard_map/psum | solution.py:57
  331.3 2.4 copy-start.2
Sparse Core Ops, SparseCore 0:
  10.0 91.4 all-gather.6
  104.2 106.9 all-gather.10
  213.9 86.9 all-gather.8
  312.3 19.0 all-reduce.2
  333.9 89.9 all-gather.12
  426.4 87.4 all-gather.14
  516.5 106.9 all-gather.16
  635.4 18.5 all-reduce.4
where the time goes:
time: 665 us
  waiting for transfers between devices  603 us (91%)
  matrix products  37.1 us (6%)
  between operations  13.5 us (2%)
  other arithmetic  10.8 us (2%)
    all_gather x1, waiting for transfers between devices, shards(): down_two = lax.all_gather(down_second, 'fs', axis=1, tiled=True)  110 us
    all_gather x1, waiting for transfers between devices, shards(): down_whole = lax.all_gather(down_first, 'fs', axis=1, tiled=True)  103 us
    all_gather x1, waiting for transfers between devices, shards(): lax.all_gather(gate_first, 'fs', axis=0, tiled=True)  90.9 us
    all_gather x1, waiting for transfers between devices, shards(): lax.all_gather(up_first, 'fs', axis=0, tiled=True)  89.7 us
    all_gather x1, waiting for transfers between devices, shards(): lax.all_gather(gate_second, 'fs', axis=0, tiled=True)  87.8 us
    all_gather x1, waiting for transfers between devices, shards(): lax.all_gather(up_second, 'fs', axis=0, tiled=True)  82.9 us
    psum x1, waiting for transfers between devices, shards(): lax.psum(partial_two.astype(jnp.bfloat16), 'tp').astype(jnp.float32)  18.7 us
    psum x1, waiting for transfers between devices, shards(): lax.psum(partial_value.astype(jnp.bfloat16), 'tp').astype(jnp.float32)  17 us
  transfers between devices with their start and end apart: 8, of which 8 were waited for; matrix products, arithmetic and copies ran while one was open for 3% of the time, Pallas kernels for 0%

commit v1 on v0

--- a/solution.py
+++ b/solution.py
@@ -52,7 +52,8 @@
         ),
     )
     hidden_two = (jax.nn.silu(gate_two) * up_two).astype(jnp.bfloat16)
-    down_two = lax.all_gather(down_second, "fs", axis=1, tiled=True)
+    make_the_tokens = lambda q_in, dev_axis: jnp.concatenate(lax.all_gather(q_in, dev_axis), axis=1)
+    down_two = make_the_tokens(down_second, "fs")
     partial_two = jnp.dot(hidden_two, down_two, preferred_element_type=jnp.float32)
     second_sum = lax.psum(partial_two.astype(jnp.bfloat16), "tp").astype(jnp.float32)
     return (middle + 0.5 * second_sum).astype(jnp.bfloat16)

time: 665 us -> 637 us (0.958)
  waiting for transfers between devices: 603 us -> 566 us
  local copies, waits for them, and re-layouts: 0.02 us -> 8.58 us
    all_gather x1, waiting for transfers between devices: 110 us -> 76.8 us  [shards(): lax.all_gather(q_in, dev_axis)]
    reshape x0 -> x1, local copies, waits for them, and re-layouts: none -> 8.56 us  [shards(): jnp.concatenate(lax.all_gather(q_in, dev_axis), axis=1)]
    all_gather x1, waiting for transfers between devices: 103 us -> 110 us  [shards(): down_whole = lax.all_gather(down_first, 'fs', axis=1, tiled=True)]
    all_gather x1, waiting for transfers between devices: 89.7 us -> 83 us  [shards(): lax.all_gather(up_first, 'fs', axis=0, tiled=True)]
  transfers between devices with their start and end apart: 8 -> 8, of which waited for: 8 -> 8; matrix products, arithmetic and copies ran while one was open for 3% -> 6% of each run, Pallas kernels for 0% -> 0%
where the time goes in v1:
time: 637 us
  waiting for transfers between devices  566 us (89%)
  matrix products  37 us (6%)
  between operations  13.5 us (2%)
  other arithmetic  10.8 us (2%)
  local copies, waits for them, and re-layouts  8.58 us (1%)
    all_gather x1, waiting for transfers between devices, shards(): down_whole = lax.all_gather(down_first, 'fs', axis=1, tiled=True)  110 us
    all_gather x1, waiting for transfers between devices, shards(): lax.all_gather(gate_first, 'fs', axis=0, tiled=True)  90.3 us
    all_gather x1, waiting for transfers between devices, shards(): lax.all_gather(gate_second, 'fs', axis=0, tiled=True)  87.8 us
    all_gather x1, waiting for transfers between devices, shards(): lax.all_gather(up_second, 'fs', axis=0, tiled=True)  83.1 us
    all_gather x1, waiting for transfers between devices, shards(): lax.all_gather(up_first, 'fs', axis=0, tiled=True)  83 us
    all_gather x1, waiting for transfers between devices, shards(): lax.all_gather(q_in, dev_axis)  76.8 us
    psum x1, waiting for transfers between devices, shards(): lax.psum(partial_two.astype(jnp.bfloat16), 'tp').astype(jnp.float32)  19.2 us
    dot_general x2, matrix products, make_folder(): jnp.dot(normed, pieces[0], preferred_element_type=jnp.float32)  14.2 us
  transfers between devices with their start and end apart: 8, of which 8 were waited for; matrix products, arithmetic and copies ran while one was open for 6% of the time, Pallas kernels for 0%

profile of v1, /device:TPU:0, one launch (start us, length us, event | category | flops | bytes accessed | tf_op | source)
XLA Modules:
  0.0 636.8 jit_solution(6115329857536967361)
XLA Ops:
  6.5 0.7 all-gather.8.cloned.1.call-update
  7.3 0.7 all-gather.10.cloned.1.call-update
  8.1 0.7 all-gather.12.cloned.1.call-update
  8.8 0.5 all-gather.18.cloned.1.call-update
  9.4 1.8 fusion.1
  11.2 90.3 %all-gather.8.cloned.1.call-done = bf16[2048,1408]{1,0:T(8,128)(2,1)} async-done(((bf16[128,1408]{1,0:T(8,128)(2,1)}), bf16[2048,1408]{1,0:T(8,128)(2,1)}) %all-gather.8.cloned.1.call-update) | async-done | bytes 5767184 | tf_op jit(solution)/shard_map/all_gather | solution.py:37
  101.5 7.2 %fusion.8 = f32[384,1408]{1,0:T(8,128)} fusion(bf16[2048,1408]{1,0:T(8,128)(2,1)} %all-gather.8.cloned.1.call-done, bf16[384,2048]{1,0:T(8,128)(2,1)} %param.10, f32[2048]{0:T(1024)} %param.12, f32[384]{0:T(512)S(1)} %add_rsqrt_fusion.1), kind=kOutput, calls=%fused_computation.16 | convolution fusion | flops 2217738240 | bytes 9512448 | tf_op jit(solution)/shard_map/dot_general | solution.py:16
  108.7 83.0 %all-gather.10.cloned.1.call-done = bf16[2048,1408]{1,0:T(8,128)(2,1)} async-done(((bf16[128,1408]{1,0:T(8,128)(2,1)}), bf16[2048,1408]{1,0:T(8,128)(2,1)}) %all-gather.10.cloned.1.call-update) | async-done | bytes 5767184 | tf_op jit(solution)/shard_map/all_gather | solution.py:38
  191.7 109.7 %all-gather.12.cloned.1.call-done = bf16[1408,2048]{1,0:T(8,128)(2,1)} async-done(((bf16[1408,128]{1,0:T(8,128)(2,1)}), bf16[1408,2048]{1,0:T(8,128)(2,1)}) %all-gather.12.cloned.1.call-update) | async-done | bytes 5767184 | tf_op jit(solution)/shard_map/all_gather | solution.py:42
  301.4 11.2 %convolution_convert_fusion.1 = bf16[384,2048]{1,0:T(8,128)(2,1)} fusion(bf16[1408,2048]{1,0:T(8,128)(2,1)} %all-gather.12.cloned.1.call-done, bf16[2048,1408]{1,0:T(8,128)(2,1)} %all-gather.10.cloned.1.call-done, f32[384,1408]{1,0:T(8,128)} %fusion.8, bf16[384,2048]{1,0:T(8,128)(2,1)S(1)} %copy-done, f32[2048]{0:T(1024)S(1)} %copy-done.4, ...), kind=kOutput, calls=%fused_computation.15 | convolution fusion | flops 4436361216 | bytes 16852480 | tf_op jit(solution)/shard_map/dot_general | solution.py:43
  312.7 0.5 all-gather.14.cloned.1.call-update
  313.3 0.7 all-gather.16.cloned.1.call-update
  314.0 0.2 all-reduce.5.cloned.1.call-start
  314.2 76.8 %all-gather.18.cloned.1.call-done = bf16[22528,128]{1,0:T(8,128)(2,1)} async-done(((bf16[1408,128]{1,0:T(8,128)(2,1)}), bf16[22528,128]{1,0:T(8,128)(2,1)}) %all-gather.18.cloned.1.call-update) | async-done | bytes 5767184 | tf_op jit(solution)/shard_map/all_gather | solution.py:55
  391.0 8.6 %copy.11 = bf16[1408,16,128]{0,2,1:T(8,128)(2,1)} copy(bf16[1408,16,128]{2,0,1:T(8,128)(2,1)} %bitcast.12) | data formatting | bytes 11534336 | tf_op jit(solution)/shard_map/reshape | solution.py:55
  399.5 12.7 %all-reduce.3.cloned.1.call-done = bf16[384,2048]{1,0:T(8,128)(2,1)} async-done(((bf16[384,2048]{1,0:T(8,128)(2,1)}), bf16[384,2048]{1,0:T(8,128)(2,1)}) %all-reduce.3.cloned.1.call-update) | async-done | bytes 1572880 | tf_op jit(solution)/shard_map/psum | solution.py:44
  412.2 2.4 multiply_reduce_fusion
  414.7 2.2 multiply_convert_fusion
  416.9 87.8 %all-gather.14.cloned.1.call-done = bf16[2048,1408]{1,0:T(8,128)(2,1)} async-done(((bf16[128,1408]{1,0:T(8,128)(2,1)}), bf16[2048,1408]{1,0:T(8,128)(2,1)}) %all-gather.14.cloned.1.call-update) | async-done | bytes 5767184 | tf_op jit(solution)/shard_map/all_gather | solution.py:50
  504.7 7.1 %fusion.12 = f32[384,1408]{1,0:T(8,128)} fusion(bf16[384,2048]{1,0:T(8,128)(2,1)} %multiply_convert_fusion, bf16[2048,1408]{1,0:T(8,128)(2,1)} %all-gather.14.cloned.1.call-done), kind=kOutput, calls=%fused_computation.21 | convolution fusion | flops 2214592512 | bytes 9502720 | tf_op jit(solution)/shard_map/dot_general | solution.py:16
  511.8 83.1 %all-gather.16.cloned.1.call-done = bf16[2048,1408]{1,0:T(8,128)(2,1)} async-done(((bf16[128,1408]{1,0:T(8,128)(2,1)}), bf16[2048,1408]{1,0:T(8,128)(2,1)}) %all-gather.16.cloned.1.call-update) | async-done | bytes 5767184 | tf_op jit(solution)/shard_map/all_gather | solution.py:51
  594.9 11.6 %convolution_convert_fusion = bf16[384,2048]{1,0:T(8,128)(2,1)} fusion(bf16[1408,2048]{0,1:T(8,128)(2,1)} %bitcast.13, bf16[384,2048]{1,0:T(8,128)(2,1)} %multiply_convert_fusion, bf16[2048,1408]{1,0:T(8,128)(2,1)} %all-gather.16.cloned.1.call-done, f32[384,1408]{1,0:T(8,128)} %fusion.12), kind=kOutput, calls=%fused_computation.14 | convolution fusion | flops 4433215488 | bytes 16842752 | tf_op jit(solution)/shard_map/dot_general | solution.py:57
  606.5 19.2 %all-reduce.5.cloned.1.call-done = bf16[384,2048]{1,0:T(8,128)(2,1)} async-done(((bf16[384,2048]{1,0:T(8,128)(2,1)}), bf16[384,2048]{1,0:T(8,128)(2,1)}) %all-reduce.5.cloned.1.call-update) | async-done | bytes 1572880 | tf_op jit(solution)/shard_map/psum | solution.py:58
  625.7 4.3 add_convert_fusion
  (21 shorter events, 0.3 us)
Async XLA Ops:
  6.5 95.0 %all-gather.8.cloned.1.call-start = ((), (), s32[]{:S(2)}) async-start(), calls=%async_computation | async-start | bytes 6127616 | tf_op jit(solution)/shard_map/all_gather | solution.py:37
  7.3 184.4 %all-gather.10.cloned.1.call-start = ((), (), s32[]{:S(2)}) async-start(), calls=%async_computation.1 | async-start | bytes 6127616 | tf_op jit(solution)/shard_map/all_gather | solution.py:38
  8.0 293.4 %all-gather.12.cloned.1.call-start = ((), (), s32[]{:S(2)}) async-start(), calls=%async_computation.2 | async-start | bytes 6127616 | tf_op jit(solution)/shard_map/all_gather | solution.py:42
  8.7 382.2 %all-gather.18.cloned.1.call-start = ((), (), s32[]{:S(2)}) async-start(), calls=%async_computation.7 | async-start | bytes 6127616 | tf_op jit(solution)/shard_map/all_gather | solution.py:55
  9.3 402.9 %all-reduce.3.cloned.1.call-start = ((), (), s32[]{:S(2)}) async-start(), calls=%async_computation.3 | async-start | bytes 3145728 | tf_op jit(solution)/shard_map/psum | solution.py:44
  11.2 290.2 %copy-start = (bf16[384,2048]{1,0:T(8,128)(2,1)S(1)}, bf16[384,2048]{1,0:T(8,128)(2,1)}, u32[]{:S(2)}) copy-start(bf16[384,2048]{1,0:T(8,128)(2,1)} %param.10) | copy-start | bytes 4718596
  11.2 290.2 %copy-start.4 = (f32[2048]{0:T(1024)S(1)}, f32[2048]{0:T(1024)}, u32[]{:S(2)}) copy-start(f32[2048]{0:T(1024)} %param.12) | copy-start | bytes 24580
  312.6 192.1 %all-gather.14.cloned.1.call-start = ((), (), s32[]{:S(2)}) async-start(), calls=%async_computation.4 | async-start | bytes 6127616 | tf_op jit(solution)/shard_map/all_gather | solution.py:50
  313.2 281.7 %all-gather.16.cloned.1.call-start = ((), (), s32[]{:S(2)}) async-start(), calls=%async_computation.5 | async-start | bytes 6127616 | tf_op jit(solution)/shard_map/all_gather | solution.py:51
  314.0 311.7 %all-reduce.5.cloned.1.call-start = ((), (), s32[]{:S(2)}) async-start(), calls=%async_computation.6 | async-start | bytes 3145728 | tf_op jit(solution)/shard_map/psum | solution.py:58
  391.0 21.3 %copy-start.1 = (bf16[384,2048]{1,0:T(8,128)(2,1)S(1)}, bf16[384,2048]{1,0:T(8,128)(2,1)}, u32[]{:S(2)}) copy-start(bf16[384,2048]{1,0:T(8,128)(2,1)} %param.11) | copy-start | bytes 4718596
  399.5 15.1 %copy-start.3 = (f32[2048]{0:T(1024)S(1)}, f32[2048]{0:T(1024)}, u32[]{:S(2)}) copy-start(f32[2048]{0:T(1024)} %param.16) | copy-start | bytes 24580
  412.2 2.4 copy-start.2
Sparse Core Ops, SparseCore 0:
  10.0 91.4 all-gather.7
  104.2 87.4 all-gather.9
  194.4 106.9 all-gather.11
  303.9 86.9 all-gather.17
  393.1 19.0 all-reduce.2
  414.8 89.9 all-gather.13
  507.4 87.4 all-gather.15
  606.6 19.0 all-reduce.4
